TPU v7x, 32 devices: a whole 2x2x4 slice. The times are simulated.
32 devices in a mesh: ep: 16 (over z, y, x), tp: 2 (over core).
Axes of the slice: x: 2, y: 2, z: 4, core: 2. Of those that a mesh axis runs over, the one named last changes fastest.
Arguments:
- hidden_in: bfloat16 [512, 2048], P('ep'), may hold values from -6 to 6
- past_lengths: int32 [512], P('ep'), may hold values from 1 to 1023, as said below
- key_cache: bfloat16 [512, 1024, 256], P('ep', None, 'tp'), may hold values from -512 to 512
- value_cache: bfloat16 [512, 1024, 256], P('ep', None, 'tp'), may hold values from -6 to 6
- attn_gain: float32 [2048], replicated, may hold values from 0.1 to 1.9
- w_query: bfloat16 [2048, 2048], P(None, 'tp'), may hold values from -0.125 to 0.125
- w_key: bfloat16 [2048, 256], P(None, 'tp'), may hold values from -0.125 to 0.125
- w_value: bfloat16 [2048, 256], P(None, 'tp'), may hold values from -0.125 to 0.125
- lambdas: float32 [16], P('tp'), may hold values from 0.3 to 0.8
- head_gain: float32 [128], replicated, may hold values from 0.1 to 1.9
- w_out: bfloat16 [2048, 2048], P('tp'), may hold values from -0.125 to 0.125
- ffn_gain: float32 [2048], replicated, may hold values from 0.1 to 1.9
- route_ids: int32 [512, 2], P('ep'), may hold values from 0 to 7, all different within a row; in each aligned block of 32 rows (0 to 31, 32 to 63, ...) at most 16 rows name the same one
- route_weights: float32 [512, 2], P('ep'), may hold values from 0.2 to 1
- expert_gate: bfloat16 [16, 2048, 704], P('ep', None, 'tp'), may hold values from -0.125 to 0.125
- expert_up: bfloat16 [16, 2048, 704], P('ep', None, 'tp'), may hold values from -0.125 to 0.125
- expert_down: bfloat16 [16, 704, 2048], P('ep', None, 'tp'), may hold values from -1.25 to 1.25
- gate_vector: bfloat16 [2048], replicated, may hold values from -0.125 to 0.125
- dense_gate: bfloat16 [2048, 5632], P(None, ('ep', 'tp')), may hold values from -0.125 to 0.125
- dense_up: bfloat16 [2048, 5632], P(None, ('ep', 'tp')), may hold values from -0.125 to 0.125
- dense_down: bfloat16 [5632, 2048], P('ep', 'tp'), may hold values from -0.625 to 0.625
Outputs:
- mixed_out: bfloat16 [512, 2048], P('ep', 'tp')
- new_keys: bfloat16 [512, 256], P('ep', 'tp')
- new_values: bfloat16 [512, 256], P('ep', 'tp')
Inputs may be any that keep to these rules, and one draw needn't show every extreme that they name: `past_lengths`: the new token of a sequence stands at this position; some sequence has 1023 cached positions in every draw. `route_ids`: each row names 2 different experts; among the rows of one index of ep no expert is named more than 16 times, a bound that some block reaches in every draw.
All inputs are finite; a program needn't handle non-finite values.
Results may differ from a plain program's by a relative error of at most 0.02.
The roundings to bfloat16 on the way count: a program that leaves them out, or rounds other values in their place, can miss the bound.
Values may be sent and summed in bfloat16 or wider, within the bound.
A program may use at most 128 MiB of HBM per device.

v0:
```python
import jax
import jax.numpy as jnp
from jax import lax
from jax.sharding import PartitionSpec as P

HEAD_DIM = 64
VALUE_DIM = 128
norm_eps = 1e-05
rope_base = 10000.0


def rms_rows(values, scales):
    values = values.astype(jnp.float32)
    return values * lax.rsqrt(jnp.mean(values * values, axis=-1, keepdims=True) + norm_eps) * scales


def rotary(values, position):
    middle = values.shape[-1] // 2
    inverse = rope_base ** (-jnp.arange(middle, dtype=jnp.float32) / middle)
    angles = position.astype(jnp.float32)[:, None] * inverse[None, :]
    cosine = jnp.cos(angles)[:, None, None, :]
    sine_part = jnp.sin(angles)[:, None, None, :]
    leading, second = (values[..., :middle], values[..., middle:])
    return jnp.concatenate(
        [leading * cosine - second * sine_part, second * cosine + leading * sine_part], axis=-1
    )


def per_device(
    hidden_in,
    past_lengths,
    key_cache,
    value_cache,
    attn_gain,
    w_query,
    w_key,
    w_value,
    lambdas,
    head_gain,
    w_out,
    ffn_gain,
    route_ids,
    route_weights,
    expert_gate,
    expert_up,
    expert_down,
    gate_vector,
    dense_gate,
    dense_up,
    dense_down,
):
    batch_rows = hidden_in.shape[0]
    model_width = hidden_in.shape[1]
    tp_count = lax.axis_size("tp")
    ep_count = lax.axis_size("ep")
    tp_rank = lax.axis_index("tp")
    half_width = model_width // tp_count
    heads_here = lambdas.shape[0]
    kv_here = w_key.shape[1] // (2 * HEAD_DIM)
    per_key = heads_here // kv_here
    scale_qk = HEAD_DIM ** (-0.5)
    normed = rms_rows(hidden_in, attn_gain).astype(jnp.bfloat16)
    queries = rotary(
        jnp.dot(normed, w_query, preferred_element_type=jnp.float32).reshape(
            batch_rows, heads_here, 2, HEAD_DIM
        ),
        past_lengths,
    ).astype(jnp.bfloat16)
    key_new = rotary(
        jnp.dot(normed, w_key, preferred_element_type=jnp.float32).reshape(
            batch_rows, kv_here, 2, HEAD_DIM
        ),
        past_lengths,
    ).astype(jnp.bfloat16)
    value_new = jnp.dot(normed, w_value, preferred_element_type=jnp.float32).astype(jnp.bfloat16)
    grouped = queries.reshape(batch_rows, kv_here, per_key, 2, HEAD_DIM)
    own_score = (
        jnp.einsum("sgamd,sgmd->sgam", grouped, key_new, preferred_element_type=jnp.float32)
        * scale_qk
    )
    value_rows = value_new.reshape(batch_rows, kv_here, 1, 1, VALUE_DIM).astype(jnp.float32)
    start_state = (
        own_score,
        jnp.ones_like(own_score),
        jnp.broadcast_to(value_rows, own_score.shape + (VALUE_DIM,)),
    )
    cache_len = key_cache.shape[1]
    span_len = min(256, cache_len)
    spans_needed = (jnp.max(past_lengths) + span_len - 1) // span_len

    def visit(block_index, carried):
        running, totals, summed = carried
        offset = block_index * span_len
        key_rows = lax.dynamic_slice_in_dim(key_cache, offset, span_len, 1).reshape(
            batch_rows, span_len, kv_here, 2, HEAD_DIM
        )
        cached = lax.dynamic_slice_in_dim(value_cache, offset, span_len, 1).reshape(
            batch_rows, span_len, kv_here, VALUE_DIM
        )
        scores = (
            jnp.einsum("sgamd,slgmd->sgaml", grouped, key_rows, preferred_element_type=jnp.float32)
            * scale_qk
        )
        usable = (offset + jnp.arange(span_len))[None, :] < past_lengths[:, None]
        scores = jnp.where(usable[:, None, None, None, :], scores, -jnp.inf)
        raised = jnp.maximum(running, jnp.max(scores, axis=-1))
        fading = jnp.exp(running - raised)
        weights = jnp.exp(scores - raised[..., None])
        totals = totals * fading + jnp.sum(weights, axis=-1)
        summed = summed * fading[..., None] + jnp.einsum(
            "sgaml,slge->sgame",
            weights.astype(jnp.bfloat16),
            cached,
            preferred_element_type=jnp.float32,
        )
        return (raised, totals, summed)

    running, totals, summed = lax.fori_loop(0, spans_needed, visit, start_state)
    mapped = summed / totals[..., None]
    head_mix = mapped[..., 0, :] - lambdas.reshape(1, kv_here, per_key, 1) * mapped[..., 1, :]
    head_out = rms_rows(head_mix, head_gain).astype(jnp.bfloat16).reshape(batch_rows, -1)
    attn_out = lax.psum(
        jnp.dot(head_out, w_out, preferred_element_type=jnp.float32).astype(jnp.bfloat16), "tp"
    )
    residual = hidden_in.astype(jnp.float32) + attn_out.astype(jnp.float32)
    moe_in = rms_rows(residual, ffn_gain).astype(jnp.bfloat16)
    mix_gate = jax.nn.sigmoid(
        jnp.dot(moe_in, gate_vector, preferred_element_type=jnp.float32)
    ).astype(jnp.bfloat16)
    top_count = route_ids.shape[1]
    experts = ep_count // 2
    capacity = max(2, 2 * batch_rows * top_count // experts)
    flat_ids = route_ids.reshape(-1)
    matches = (flat_ids[:, None] == jnp.arange(experts)[None, :]).astype(jnp.int32)
    earlier = jnp.sum((jnp.cumsum(matches, axis=0) - matches) * matches, axis=1)
    slot_of = flat_ids * capacity + earlier
    placing = (jnp.arange(experts * capacity)[:, None] == slot_of[None, :]).astype(jnp.float32)
    repeated = jnp.repeat(moe_in, top_count, axis=0)
    packed = jnp.dot(
        placing.astype(jnp.bfloat16), repeated, preferred_element_type=jnp.float32
    ).astype(jnp.bfloat16)
    outgoing = jnp.broadcast_to(
        packed.reshape(experts, 1, capacity, model_width), (experts, 2, capacity, model_width)
    ).reshape(ep_count, capacity, model_width)
    arrived = lax.all_to_all(outgoing, "ep", split_axis=0, concat_axis=0, tiled=True)
    leading = arrived.shape[:2]
    flat_rows = arrived.reshape(-1, model_width)
    gate_pre = jnp.dot(flat_rows, expert_gate[0], preferred_element_type=jnp.float32)
    up_pre = jnp.dot(flat_rows, expert_up[0], preferred_element_type=jnp.float32)
    inner_act = (jax.nn.silu(gate_pre) * up_pre).astype(jnp.bfloat16)
    inner_act = lax.all_gather(inner_act, "tp", axis=1, tiled=True)
    partial_value = jnp.dot(inner_act, expert_down[0], preferred_element_type=jnp.float32).reshape(
        leading + (half_width,)
    )
    returned = lax.all_to_all(
        partial_value.astype(jnp.bfloat16), "ep", split_axis=0, concat_axis=0, tiled=True
    ).astype(partial_value.dtype)
    paired = jnp.sum(returned.reshape(experts, 2, capacity, half_width), axis=1).reshape(
        experts * capacity, half_width
    )
    weighted = (
        (placing * route_weights.reshape(1, -1))
        .reshape(experts * capacity, batch_rows, top_count)
        .sum(axis=2)
    )
    moe_out = jnp.einsum("ct,cd->td", weighted, paired, precision=lax.Precision.HIGHEST)
    rows_all, gates_all = (
        lax.all_gather(moe_in, "ep", axis=0, tiled=True),
        lax.all_gather(mix_gate, "ep", axis=0, tiled=True),
    )
    local_pre = jnp.dot(rows_all, dense_gate, preferred_element_type=jnp.float32)
    local_up = jnp.dot(rows_all, dense_up, preferred_element_type=jnp.float32)
    local_act = (jax.nn.silu(local_pre) * local_up).astype(jnp.bfloat16)
    dense_act = lax.all_gather(local_act, "tp", axis=1, tiled=True)
    gate_rows = gates_all.astype(jnp.float32)
    dense_out = lax.psum_scatter(
        jnp.dot(dense_act, dense_down, preferred_element_type=jnp.float32) * gate_rows[:, None],
        "ep",
        scatter_dimension=0,
        tiled=True,
    )
    own_residual = lax.dynamic_slice_in_dim(residual, tp_rank * half_width, half_width, 1)
    mixed_out = (own_residual + moe_out + dense_out).astype(jnp.bfloat16)
    return (mixed_out, key_new.reshape(batch_rows, -1), value_new)


def solution(mesh):
    return jax.shard_map(
        per_device,
        mesh=mesh,
        in_specs=(
            P("ep", None),
            P("ep"),
            P("ep", None, "tp"),
            P("ep", None, "tp"),
            P(),
            P(None, "tp"),
            P(None, "tp"),
            P(None, "tp"),
            P("tp"),
            P(),
            P("tp", None),
            P(),
            P("ep", None),
            P("ep", None),
            P("ep", None, "tp"),
            P("ep", None, "tp"),
            P("ep", None, "tp"),
            P(),
            P(None, ("ep", "tp")),
            P(None, ("ep", "tp")),
            P("ep", "tp"),
        ),
        out_specs=(P("ep", "tp"), P("ep", "tp"), P("ep", "tp")),
        check_vma=False,
    )
```

profile of v0, /device:TPU:0, one launch (start us, length us, event | category | flops | bytes accessed | tf_op | source)
XLA Modules:
  0.0 262.9 jit_solution(17510185976092909314)
XLA Ops:
  7.2 1.4 fusion.67
  10.4 1.4 fusion.62
  11.9 3.2 %fusion.60 = f32[32,1024]{1,0:T(8,128)S(1)} fusion(bf16[2048,1024]{1,0:T(8,128)(2,1)} %param.28, bf16[32,2048]{1,0:T(8,128)(2,1)} %param.23, f32[2048]{0:T(1024)} %param.27, f32[32]{0:T(128)S(1)} %add_rsqrt_fusion.2), kind=kOutput, calls=%fused_computation.98 | convolution fusion | flops 134479872 | bytes 4464768 | tf_op jit(solution)/shard_map/dot_general | solution.py:64
  19.8 36.4 %while.14 = (s32[]{:T(128)}, f32[32,1,8,2]{2,3,0,1:T(2,128)}, f32[32,1,8,2]{2,3,0,1:T(2,128)}, f32[32,1,8,2,128]{4,2,3,0,1:T(8,128)}, s32[]{:T(128)}, /*index=5*...) while((s32[]{:T(128)}, f32[32,1,8,2]{2,3,0,1:T(2,128)}, ...), condition=%wide.region_5.6_spmd, body=%wide.region_2.5_spmd.sunk | while | flops 51390212 | bytes 16918980 | solution.py:118
  19.8 3.2 %constant_dynamic-slice_fusion.2 = bf16[32,256,128]{2,1,0:T(8,128)(2,1)} fusion(bf16[32,1024,128]{2,1,0:T(8,128)(2,1)} %get-tuple-element.224, s32[]{:T(128)S(6)} %select_n.25), kind=kLoop, calls=%fused_computation.22.clone.1 | loop fusion | bytes 4194308 | tf_op jit(solution)/shard_map/while/body/dynamic_slice | solution.py:94
  23.0 3.3 %copy.81 = bf16[32,256,128]{1,2,0:T(8,128)(2,1)S(1)} copy(bf16[32,256,128]{2,1,0:T(8,128)(2,1)} %constant_dynamic-slice_fusion.2) | data formatting | bytes 4194304 | tf_op jit(solution)/shard_map/while/body/dynamic_slice | solution.py:94
  27.1 1.4 fusion.98
  28.5 2.1 fusion.101
  32.0 3.2 %constant_dynamic-slice_fusion.2 = bf16[32,256,128]{2,1,0:T(8,128)(2,1)} fusion(bf16[32,1024,128]{2,1,0:T(8,128)(2,1)} %get-tuple-element.224, s32[]{:T(128)S(6)} %select_n.25), kind=kLoop, calls=%fused_computation.22.clone.1 | loop fusion | bytes 4194308 | tf_op jit(solution)/shard_map/while/body/dynamic_slice | solution.py:94
  35.1 3.3 %copy.81 = bf16[32,256,128]{1,2,0:T(8,128)(2,1)S(1)} copy(bf16[32,256,128]{2,1,0:T(8,128)(2,1)} %constant_dynamic-slice_fusion.2) | data formatting | bytes 4194304 | tf_op jit(solution)/shard_map/while/body/dynamic_slice | solution.py:94
  39.2 1.4 fusion.98
  40.7 2.1 fusion.101
  44.1 3.2 %constant_dynamic-slice_fusion.2 = bf16[32,256,128]{2,1,0:T(8,128)(2,1)} fusion(bf16[32,1024,128]{2,1,0:T(8,128)(2,1)} %get-tuple-element.224, s32[]{:T(128)S(6)} %select_n.25), kind=kLoop, calls=%fused_computation.22.clone.1 | loop fusion | bytes 4194308 | tf_op jit(solution)/shard_map/while/body/dynamic_slice | solution.py:94
  47.3 3.3 %copy.81 = bf16[32,256,128]{1,2,0:T(8,128)(2,1)S(1)} copy(bf16[32,256,128]{2,1,0:T(8,128)(2,1)} %constant_dynamic-slice_fusion.2) | data formatting | bytes 4194304 | tf_op jit(solution)/shard_map/while/body/dynamic_slice | solution.py:94
  51.3 1.4 fusion.98
  52.8 2.1 fusion.101
  56.2 1.1 broadcast_divide_fusion
  59.1 3.7 %convolution_convert_fusion.1 = bf16[32,2048]{1,0:T(8,128)(2,1)} fusion(bf16[1024,2048]{1,0:T(8,128)(2,1)} %param.33, f32[4,8,8,128]{3,2,1,0:T(8,128)S(1)} %bitcast.178, f32[4,8,8,128]{3,2,1,0:T(8,128)S(1)} %bitcast.180, f32[4,8,8,128]{3,2,1,0:T(8,128)S(1)} %bitcast.179, f32[1024]{0:T(1024)S(1)} %get-tuple-element.126, f32[1024]{0:T(1024)S(1)} %get-tuple-element.127), kind=kOutput, calls=%fused_computation.24 | convolution fusion | flops 134447104 | bytes 4726784 | tf_op jit(solution)/shard_map/dot_general | solution.py:123
  62.9 32.9 %all-reduce.3.cloned.1.call-done = bf16[32,2048]{1,0:T(8,128)(2,1)} async-done(((bf16[32,2048]{1,0:T(8,128)(2,1)}), bf16[32,2048]{1,0:T(8,128)(2,1)}) %all-reduce.3.cloned.1.call-update) | async-done | bytes 131088 | tf_op jit(solution)/shard_map/psum | solution.py:122
  96.9 1.6 multiply_convert_fusion
  102.9 42.2 %all-reduce = bf16[512]{0:T(512)(128)(2,1)S(1)} all-reduce(bf16[512]{0:T(512)(128)(2,1)S(1)} %dynamic-update-slice), channel_id=1, replica_groups=mesh['ep'=16,'tp'=2] {'ep'}, use_global_device_ids=true, to_apply=%add | all-reduce | flops 512 | bytes 2048
  145.1 15.5 %all-gather.2.cloned.1.call-done = bf16[512,2048]{1,0:T(8,128)(2,1)} async-done(((bf16[32,2048]{1,0:T(8,128)(2,1)}), bf16[512,2048]{1,0:T(8,128)(2,1)}) %all-gather.2.cloned.1.call-update) | async-done | bytes 2097168 | tf_op jit(solution)/shard_map/all_gather | solution.py:168
  160.6 2.6 fusion.68
  164.1 2.1 all_gather.14
  166.2 2.1 convolution_multiply_fusion.1
  168.7 38.9 %all_to_all.10 = bf16[16,16,2048]{2,1,0:T(8,128)(2,1)S(1)} all-to-all(bf16[16,16,2048]{2,1,0:T(8,128)(2,1)S(1)} %bitcast.170), channel_id=1, replica_groups=mesh['ep'=16,'tp'=2] {'ep'}, dimensions={0} | all-to-all | bytes 2097152 | tf_op jit(solution)/shard_map/all_to_all | solution.py:145
  208.8 2.1 all_gather.12
  211.0 1.4 fusion.26
  212.4 4.3 %all-to-all-start.1 = ((bf16[16,16,1024]{2,1,0:T(8,128)(2,1)}), bf16[16,16,1024]{2,1,0:T(8,128)(2,1)S(1)}, u32[]{:S(2)}, u32[]{:S(2)}) async-start(bf16[16,16,1024]{2,1,0:T(8,128)(2,1)} %fusion.26), calls=%async_computation.1 | async-start | bytes 1048576 | tf_op jit(solution)/shard_map/all_to_all | solution.py:155
  217.8 18.3 %all-to-all-done.1 = bf16[16,16,1024]{2,1,0:T(8,128)(2,1)S(1)} async-done(((bf16[16,16,1024]{2,1,0:T(8,128)(2,1)}), bf16[16,16,1024]{2,1,0:T(8,128)(2,1)S(1)}, u32[]{:S(2)}, u32[]{:S(2)}) %all-to-all-start.1) | async-done | bytes 524320 | tf_op jit(solution)/shard_map/all_to_all | solution.py:155
  236.2 18.2 %reduce-scatter.2.cloned.1.call-done = f32[32,1024]{1,0:T(8,128)} async-done(((f32[512,1024]{1,0:T(8,128)}), f32[32,1024]{1,0:T(8,128)}) %reduce-scatter.2.cloned.1.call-update) | async-done | bytes 131088 | tf_op jit(solution)/shard_map/reduce_scatter | solution.py:176
  254.4 1.9 fusion.37
  (142 shorter events, 22.6 us)
Async XLA Ops:
  7.2 203.8 %copy-start = (bf16[1,704,1024]{2,1,0:T(8,128)(2,1)S(1)}, bf16[1,704,1024]{2,1,0:T(8,128)(2,1)}, u32[]{:S(2)}) copy-start(bf16[1,704,1024]{2,1,0:T(8,128)(2,1)} %param.39) | copy-start | bytes 4325380
  7.2 88.6 %all-reduce.3.cloned.1.call-start = ((), (), s32[]{:S(2)}) async-start(), calls=%async_computation.3 | async-start | bytes 262144 | tf_op jit(solution)/shard_map/psum | solution.py:122
  15.0 2.4 copy-start.1
  15.0 2.4 copy-start.10
  15.0 2.4 copy-start.13
  17.7 2.1 copy-start.14
  26.3 2.2 copy-start.3
  26.3 2.2 copy-start.7
  28.5 2.4 copy-start.4
  30.6 0.7 copy-start.8
  38.4 2.2 copy-start.3
  38.4 2.2 copy-start.7
  40.7 2.4 copy-start.4
  50.5 2.2 copy-start.3
  50.5 2.2 copy-start.7
  52.8 2.4 copy-start.4
  59.0 36.7 %copy-start.2 = (bf16[32,2048]{1,0:T(8,128)(2,1)S(1)}, bf16[32,2048]{1,0:T(8,128)(2,1)}, u32[]{:S(2)}) copy-start(bf16[32,2048]{1,0:T(8,128)(2,1)} %param.23) | copy-start | bytes 393220
  59.1 37.8 %copy-start.15 = (f32[2048]{0:T(1024)S(1)}, f32[2048]{0:T(1024)}, u32[]{:S(2)}) copy-start(f32[2048]{0:T(1024)} %param.34) | copy-start | bytes 24580
  59.1 39.5 %copy-start.17 = (s32[32,2]{0,1:T(2,128)S(1)}, s32[32,2]{0,1:T(2,128)}, u32[]{:S(2)}) copy-start(s32[32,2]{0,1:T(2,128)} %param.35) | copy-start | bytes 772
  59.1 39.9 %copy-start.16 = (bf16[2048]{0:T(1024)(128)(2,1)S(1)}, bf16[2048]{0:T(1024)(128)(2,1)}, u32[]{:S(2)}) copy-start(bf16[2048]{0:T(1024)(128)(2,1)} %param.40) | copy-start | bytes 12292
  59.1 39.9 %copy-start.23 = (u32[32]{0:T(128)S(1)}, u32[32]{0:T(128)}, u32[]{:S(2)}) copy-start(u32[32]{0:T(128)} %constant.84) | copy-start | bytes 388
  62.8 97.8 %copy-start.21 = (bf16[2048,176]{0,1:T(8,128)(2,1)S(1)}, bf16[2048,176]{0,1:T(8,128)(2,1)}, u32[]{:S(2)}) copy-start(bf16[2048,176]{0,1:T(8,128)(2,1)} %param.41) | copy-start | bytes 2162692
  62.9 97.7 %all-gather.2.cloned.1.call-start = ((), (), s32[]{:S(2)}) async-start(), calls=%async_computation.4 | async-start | bytes 2228224 | tf_op jit(solution)/shard_map/all_gather | solution.py:168
  98.5 155.9 %reduce-scatter.2.cloned.1.call-start = ((), (), s32[]{:S(2)}) async-start(), calls=%async_computation.5 | async-start | bytes 2228224 | tf_op jit(solution)/shard_map/reduce_scatter | solution.py:176
  160.6 2.6 copy-start.19
  160.6 2.6 copy-start.22
  163.2 2.9 %copy-start.9 = (bf16[352,1024]{1,0:T(8,128)(2,1)S(1)}, bf16[352,1024]{1,0:T(8,128)(2,1)}, u32[]{:S(2)}) copy-start(bf16[352,1024]{1,0:T(8,128)(2,1)} %param.43) | copy-start | bytes 2162692
  168.3 39.3 %copy-start.6 = (bf16[1,2048,352]{1,2,0:T(8,128)(2,1)S(1)}, bf16[1,2048,352]{1,2,0:T(8,128)(2,1)}, u32[]{:S(2)}) copy-start(bf16[1,2048,352]{1,2,0:T(8,128)(2,1)} %param.37) | copy-start | bytes 4325380
  168.7 39.5 %copy-start.20 = (bf16[1,2048,352]{1,2,0:T(8,128)(2,1)S(1)}, bf16[1,2048,352]{1,2,0:T(8,128)(2,1)}, u32[]{:S(2)}) copy-start(bf16[1,2048,352]{1,2,0:T(8,128)(2,1)} %param.38) | copy-start | bytes 4325380
  210.8 6.1 %copy-start.12 = (bf16[32,1,2,32]{3,2,0,1:T(2,128)(2,1)S(1)}, bf16[32,1,2,32]{3,2,0,1:T(2,128)(2,1)}, u32[]{:S(2)}) copy-start(bf16[32,1,2,32]{3,2,0,1:T(2,128)(2,1)} %copy-done.11) | copy-start | bytes 12292
  210.8 6.9 %copy-start.18 = (f32[32,2]{0,1:T(2,128)S(1)}, f32[32,2]{0,1:T(2,128)}, u32[]{:S(2)}) copy-start(f32[32,2]{0,1:T(2,128)} %param.36) | copy-start | bytes 772
  212.4 23.7 %all-to-all-start.1 = ((bf16[16,16,1024]{2,1,0:T(8,128)(2,1)}), bf16[16,16,1024]{2,1,0:T(8,128)(2,1)S(1)}, u32[]{:S(2)}, u32[]{:S(2)}) async-start(bf16[16,16,1024]{2,1,0:T(8,128)(2,1)} %fusion.26), calls=%async_computation.1 | async-start | bytes 1048576 | tf_op jit(solution)/shard_map/all_to_all | solution.py:155
  (6 other events, 3.9 us)
Sparse Core Ops, SparseCore 0:
  63.0 32.7 all-reduce.2
  98.6 61.9 all-gather.1
  168.4 85.9 reduce-scatter.1
where the time goes:
time: 264 us; the launch traced here: 263 us
  blocking collectives  85.2 us (32%)
  waiting for transfers between devices  84.9 us (32%)
  matrix products  30.5 us (12%)
  local copies, waits for them, and re-layouts  29 us (11%)
  between operations  15.5 us (6%)
  other arithmetic  13 us (5%)
  starting transfers between devices  4.45 us (2%)
    unnamed x1, blocking collectives  42.2 us
    all_to_all x1, blocking collectives, per_device(): lax.all_to_all(outgoing, 'ep', split_axis=0, concat_axis=0, tiled=True)  38.9 us
    psum x1, waiting for transfers between devices, per_device(): lax.psum(jnp.dot(head_out, w_out, preferred_element_type=jnp.float32).ast...  32.9 us
    dynamic_slice x6, local copies, waits for them, and re-layouts, visit(): lax.dynamic_slice_in_dim(key_cache, offset, span_len, 1)  19.3 us
    all_to_all x1, waiting for transfers between devices, per_device(): lax.all_to_all(partial_value.astype(jnp.bfloat16), 'ep', split_axis=0, co...  18.3 us
    reduce_scatter x1, waiting for transfers between devices, per_device(): lax.psum_scatter(jnp.dot(dense_act, dense_down, preferred_element_type=jn...  18.2 us
    all_gather x1, waiting for transfers between devices, per_device(): lax.all_gather(moe_in, 'ep', axis=0, tiled=True)  15.5 us
    dot_general x3, matrix products, visit(): jnp.einsum('sgaml,slge->sgame', weights.astype(jnp.bfloat16), cached, pre...  6.25 us
  transfers between devices with their start and end apart: 4, of which 4 were waited for; matrix products, arithmetic and copies ran while one was open for 3% of the time, Pallas kernels for 0%

commit v1 on v0

--- a/solution.py
+++ b/solution.py
@@ -7,6 +7,11 @@
 VALUE_DIM = 128
 norm_eps = 1e-05
 rope_base = 10000.0
+
+
+def gather_and_add(x, axis):
+    pieces = lax.all_gather(x, axis)
+    return jnp.sum(pieces, axis=0)
 
 
 def rms_rows(values, scales):
@@ -119,7 +124,7 @@
     mapped = summed / totals[..., None]
     head_mix = mapped[..., 0, :] - lambdas.reshape(1, kv_here, per_key, 1) * mapped[..., 1, :]
     head_out = rms_rows(head_mix, head_gain).astype(jnp.bfloat16).reshape(batch_rows, -1)
-    attn_out = lax.psum(
+    attn_out = gather_and_add(
         jnp.dot(head_out, w_out, preferred_element_type=jnp.float32).astype(jnp.bfloat16), "tp"
     )
     residual = hidden_in.astype(jnp.float32) + attn_out.astype(jnp.float32)

time: 264 us -> 245 us (0.928)
  waiting for transfers between devices: 84.9 us -> 52.8 us
  blocking collectives: 85.2 us -> 101 us
    psum x1 -> x0, waiting for transfers between devices: 32.9 us -> none  [per_device(): lax.psum(jnp.dot(head_out, w_out, preferred_element_type=jnp.float32).ast...]
    unnamed x1, blocking collectives: 42.2 us -> 55.7 us
  transfers between devices with their start and end apart: 4 -> 3, of which waited for: 4 -> 3; matrix products, arithmetic and copies ran while one was open for 3% -> 3% of each run, Pallas kernels for 0% -> 0%
where the time goes in v1:
time: 245 us; the launch traced here: 244 us
  blocking collectives  101 us (41%)
  waiting for transfers between devices  52.8 us (22%)
  matrix products  29.8 us (12%)
  local copies, waits for them, and re-layouts  29 us (12%)
  between operations  15.8 us (6%)
  other arithmetic  11.3 us (5%)
  starting transfers between devices  4.45 us (2%)
    unnamed x1, blocking collectives  55.7 us
    all_to_all x1, blocking collectives, per_device(): lax.all_to_all(outgoing, 'ep', split_axis=0, concat_axis=0, tiled=True)  38.9 us
    dynamic_slice x6, local copies, waits for them, and re-layouts, visit(): lax.dynamic_slice_in_dim(key_cache, offset, span_len, 1)  19.2 us
    reduce_scatter x1, waiting for transfers between devices, per_device(): lax.psum_scatter(jnp.dot(dense_act, dense_down, preferred_element_type=jn...  19.2 us
    all_to_all x1, waiting for transfers between devices, per_device(): lax.all_to_all(partial_value.astype(jnp.bfloat16), 'ep', split_axis=0, co...  18.1 us
    all_gather x1, waiting for transfers between devices, per_device(): lax.all_gather(moe_in, 'ep', axis=0, tiled=True)  15.5 us
    dot_general x3, matrix products, visit(): jnp.einsum('sgaml,slge->sgame', weights.astype(jnp.bfloat16), cached, pre...  6.24 us
  transfers between devices with their start and end apart: 3, of which 3 were waited for; matrix products, arithmetic and copies ran while one was open for 3% of the time, Pallas kernels for 0%

profile of v1, /device:TPU:0, one launch (start us, length us, event | category | flops | bytes accessed | tf_op | source)
XLA Modules:
  0.0 244.4 jit_solution(9492527208004837848)
XLA Ops:
  7.2 1.4 fusion.67
  10.4 1.4 fusion.62
  11.9 3.2 %fusion.60 = f32[32,1024]{1,0:T(8,128)S(1)} fusion(bf16[2048,1024]{1,0:T(8,128)(2,1)} %param.28, bf16[32,2048]{1,0:T(8,128)(2,1)} %param.23, f32[2048]{0:T(1024)} %param.27, f32[32]{0:T(128)S(1)} %add_rsqrt_fusion.2), kind=kOutput, calls=%fused_computation.98 | convolution fusion | flops 134479872 | bytes 4464768 | tf_op jit(solution)/shard_map/dot_general | solution.py:69
  19.9 36.4 %while.14 = (s32[]{:T(128)}, f32[32,1,8,2]{2,3,0,1:T(2,128)}, f32[32,1,8,2]{2,3,0,1:T(2,128)}, f32[32,1,8,2,128]{4,2,3,0,1:T(8,128)}, s32[]{:T(128)}, /*index=5*...) while((s32[]{:T(128)}, f32[32,1,8,2]{2,3,0,1:T(2,128)}, ...), condition=%wide.region_5.6_spmd, body=%wide.region_2.5_spmd.sunk | while | flops 51390212 | bytes 16918980 | solution.py:123
  19.9 3.1 %constant_dynamic-slice_fusion.2 = bf16[32,256,128]{2,1,0:T(8,128)(2,1)} fusion(bf16[32,1024,128]{2,1,0:T(8,128)(2,1)} %get-tuple-element.224, s32[]{:T(128)S(6)} %select_n.25), kind=kLoop, calls=%fused_computation.22.clone.1 | loop fusion | bytes 4194308 | tf_op jit(solution)/shard_map/while/body/dynamic_slice | solution.py:99
  23.0 3.3 %copy.81 = bf16[32,256,128]{1,2,0:T(8,128)(2,1)S(1)} copy(bf16[32,256,128]{2,1,0:T(8,128)(2,1)} %constant_dynamic-slice_fusion.2) | data formatting | bytes 4194304 | tf_op jit(solution)/shard_map/while/body/dynamic_slice | solution.py:99
  27.1 1.4 fusion.98
  28.5 2.1 fusion.101
  32.0 3.1 %constant_dynamic-slice_fusion.2 = bf16[32,256,128]{2,1,0:T(8,128)(2,1)} fusion(bf16[32,1024,128]{2,1,0:T(8,128)(2,1)} %get-tuple-element.224, s32[]{:T(128)S(6)} %select_n.25), kind=kLoop, calls=%fused_computation.22.clone.1 | loop fusion | bytes 4194308 | tf_op jit(solution)/shard_map/while/body/dynamic_slice | solution.py:99
  35.1 3.3 %copy.81 = bf16[32,256,128]{1,2,0:T(8,128)(2,1)S(1)} copy(bf16[32,256,128]{2,1,0:T(8,128)(2,1)} %constant_dynamic-slice_fusion.2) | data formatting | bytes 4194304 | tf_op jit(solution)/shard_map/while/body/dynamic_slice | solution.py:99
  39.2 1.4 fusion.98
  40.7 2.1 fusion.101
  44.1 3.1 %constant_dynamic-slice_fusion.2 = bf16[32,256,128]{2,1,0:T(8,128)(2,1)} fusion(bf16[32,1024,128]{2,1,0:T(8,128)(2,1)} %get-tuple-element.224, s32[]{:T(128)S(6)} %select_n.25), kind=kLoop, calls=%fused_computation.22.clone.1 | loop fusion | bytes 4194308 | tf_op jit(solution)/shard_map/while/body/dynamic_slice | solution.py:99
  47.2 3.3 %copy.81 = bf16[32,256,128]{1,2,0:T(8,128)(2,1)S(1)} copy(bf16[32,256,128]{2,1,0:T(8,128)(2,1)} %constant_dynamic-slice_fusion.2) | data formatting | bytes 4194304 | tf_op jit(solution)/shard_map/while/body/dynamic_slice | solution.py:99
  51.3 1.4 fusion.98
  52.8 2.1 fusion.101
  56.2 1.1 broadcast_divide_fusion
  59.1 3.0 %convolution_convert_fusion.1 = bf16[32,2048]{1,0:T(8,128)(2,1)S(1)} fusion(bf16[1024,2048]{1,0:T(8,128)(2,1)} %param.33, f32[4,8,8,128]{3,2,1,0:T(8,128)S(1)} %bitcast.180, f32[4,8,8,128]{3,2,1,0:T(8,128)S(1)} %bitcast.182, f32[4,8,8,128]{3,2,1,0:T(8,128)S(1)} %bitcast.181, f32[1024]{0:T(1024)S(1)} %get-tuple-element.126, f32[1024]{0:T(1024)S(1)} %get-tuple-element.127), kind=kOutput, calls=%fused_computation.24 | convolution fusion | flops 134447104 | bytes 4726784 | tf_op jit(solution)/shard_map/dot_general | solution.py:128
  62.1 2.3 all-gather
  65.5 1.1 broadcast_in_dim.20
  69.6 55.7 %all-reduce = bf16[512]{0:T(512)(128)(2,1)S(1)} all-reduce(bf16[512]{0:T(512)(128)(2,1)S(1)} %dynamic-update-slice), channel_id=1, replica_groups=mesh['ep'=16,'tp'=2] {'ep'}, use_global_device_ids=true, to_apply=%add | all-reduce | flops 512 | bytes 2048
  125.5 15.5 %all-gather.3.cloned.1.call-done = bf16[512,2048]{1,0:T(8,128)(2,1)} async-done(((bf16[32,2048]{1,0:T(8,128)(2,1)}), bf16[512,2048]{1,0:T(8,128)(2,1)}) %all-gather.3.cloned.1.call-update) | async-done | bytes 2097168 | tf_op jit(solution)/shard_map/all_gather | solution.py:173
  141.0 2.6 %fusion.68 = f32[512,176]{0,1:T(8,128)S(1)} fusion(bf16[512,2048]{1,0:T(8,128)(2,1)} %all-gather.3.cloned.1.call-done, bf16[2048,176]{0,1:T(8,128)(2,1)S(1)} %copy-done.21), kind=kOutput, calls=%fused_computation.104 | convolution fusion | flops 369098752 | bytes 3178496 | tf_op jit(solution)/shard_map/dot_general | solution.py:176
  144.5 2.1 all_gather.22
  146.5 2.1 convolution_multiply_fusion.1
  149.1 38.9 %all_to_all.10 = bf16[16,16,2048]{2,1,0:T(8,128)(2,1)S(1)} all-to-all(bf16[16,16,2048]{2,1,0:T(8,128)(2,1)S(1)} %bitcast.171), channel_id=1, replica_groups=mesh['ep'=16,'tp'=2] {'ep'}, dimensions={0} | all-to-all | bytes 2097152 | tf_op jit(solution)/shard_map/all_to_all | solution.py:150
  189.1 2.1 all_gather.20
  191.4 1.4 fusion.26
  192.7 4.4 %all-to-all-start.1 = ((bf16[16,16,1024]{2,1,0:T(8,128)(2,1)}), bf16[16,16,1024]{2,1,0:T(8,128)(2,1)S(1)}, u32[]{:S(2)}, u32[]{:S(2)}) async-start(bf16[16,16,1024]{2,1,0:T(8,128)(2,1)} %fusion.26), calls=%async_computation.1 | async-start | bytes 1048576 | tf_op jit(solution)/shard_map/all_to_all | solution.py:160
  198.2 18.1 %all-to-all-done.1 = bf16[16,16,1024]{2,1,0:T(8,128)(2,1)S(1)} async-done(((bf16[16,16,1024]{2,1,0:T(8,128)(2,1)}), bf16[16,16,1024]{2,1,0:T(8,128)(2,1)S(1)}, u32[]{:S(2)}, u32[]{:S(2)}) %all-to-all-start.1) | async-done | bytes 524320 | tf_op jit(solution)/shard_map/all_to_all | solution.py:160
  216.4 19.2 %reduce-scatter.2.cloned.1.call-done = f32[32,1024]{1,0:T(8,128)} async-done(((f32[512,1024]{1,0:T(8,128)}), f32[32,1024]{1,0:T(8,128)}) %reduce-scatter.2.cloned.1.call-update) | async-done | bytes 131088 | tf_op jit(solution)/shard_map/reduce_scatter | solution.py:181
  235.6 1.9 fusion.37
  (141 shorter events, 21.4 us)
Async XLA Ops:
  7.2 184.2 %copy-start = (bf16[1,704,1024]{2,1,0:T(8,128)(2,1)S(1)}, bf16[1,704,1024]{2,1,0:T(8,128)(2,1)}, u32[]{:S(2)}) copy-start(bf16[1,704,1024]{2,1,0:T(8,128)(2,1)} %param.39) | copy-start | bytes 4325380
  7.2 133.8 %all-gather.3.cloned.1.call-start = ((), (), s32[]{:S(2)}) async-start(), calls=%async_computation.3 | async-start | bytes 2228224 | tf_op jit(solution)/shard_map/all_gather | solution.py:173
  15.0 2.4 copy-start.1
  15.0 2.4 copy-start.10
  15.0 2.4 copy-start.13
  17.7 2.1 copy-start.14
  26.3 2.2 copy-start.3
  26.3 2.2 copy-start.7
  28.5 2.4 copy-start.4
  30.6 0.7 copy-start.8
  38.4 2.2 copy-start.3
  38.4 2.2 copy-start.7
  40.7 2.4 copy-start.4
  42.7 0.7 copy-start.8
  50.5 2.2 copy-start.3
  50.5 2.2 copy-start.7
  52.8 2.4 copy-start.4
  59.0 5.4 %copy-start.2 = (bf16[32,2048]{1,0:T(8,128)(2,1)S(1)}, bf16[32,2048]{1,0:T(8,128)(2,1)}, u32[]{:S(2)}) copy-start(bf16[32,2048]{1,0:T(8,128)(2,1)} %param.23) | copy-start | bytes 393220
  59.1 5.6 %copy-start.15 = (f32[2048]{0:T(1024)S(1)}, f32[2048]{0:T(1024)}, u32[]{:S(2)}) copy-start(f32[2048]{0:T(1024)} %param.34) | copy-start | bytes 24580
  62.1 4.5 %copy-start.17 = (s32[32,2]{0,1:T(2,128)S(1)}, s32[32,2]{0,1:T(2,128)}, u32[]{:S(2)}) copy-start(s32[32,2]{0,1:T(2,128)} %param.35) | copy-start | bytes 772
  62.1 4.9 %copy-start.16 = (bf16[2048]{0:T(1024)(128)(2,1)S(1)}, bf16[2048]{0:T(1024)(128)(2,1)}, u32[]{:S(2)}) copy-start(bf16[2048]{0:T(1024)(128)(2,1)} %param.40) | copy-start | bytes 12292
  62.1 4.9 %copy-start.23 = (u32[32]{0:T(128)S(1)}, u32[32]{0:T(128)}, u32[]{:S(2)}) copy-start(u32[32]{0:T(128)} %constant.86) | copy-start | bytes 388
  62.1 78.8 %copy-start.21 = (bf16[2048,176]{0,1:T(8,128)(2,1)S(1)}, bf16[2048,176]{0,1:T(8,128)(2,1)}, u32[]{:S(2)}) copy-start(bf16[2048,176]{0,1:T(8,128)(2,1)} %param.41) | copy-start | bytes 2162692
  65.4 170.2 %reduce-scatter.2.cloned.1.call-start = ((), (), s32[]{:S(2)}) async-start(), calls=%async_computation.4 | async-start | bytes 2228224 | tf_op jit(solution)/shard_map/reduce_scatter | solution.py:181
  141.0 2.6 %copy-start.19 = (bf16[512,2048]{1,0:T(8,128)(2,1)S(1)}, bf16[512,2048]{1,0:T(8,128)(2,1)}, u32[]{:S(2)}) copy-start(bf16[512,2048]{1,0:T(8,128)(2,1)} %all-gather.3.cloned.1.call-done) | copy-start | bytes 6291460
  141.0 2.6 %copy-start.22 = (bf16[2048,176]{0,1:T(8,128)(2,1)S(1)}, bf16[2048,176]{0,1:T(8,128)(2,1)}, u32[]{:S(2)}) copy-start(bf16[2048,176]{0,1:T(8,128)(2,1)} %param.42) | copy-start | bytes 2162692
  143.6 2.9 %copy-start.9 = (bf16[352,1024]{1,0:T(8,128)(2,1)S(1)}, bf16[352,1024]{1,0:T(8,128)(2,1)}, u32[]{:S(2)}) copy-start(bf16[352,1024]{1,0:T(8,128)(2,1)} %param.43) | copy-start | bytes 2162692
  148.6 39.3 %copy-start.6 = (bf16[1,2048,352]{1,2,0:T(8,128)(2,1)S(1)}, bf16[1,2048,352]{1,2,0:T(8,128)(2,1)}, u32[]{:S(2)}) copy-start(bf16[1,2048,352]{1,2,0:T(8,128)(2,1)} %param.37) | copy-start | bytes 4325380
  149.0 39.5 %copy-start.20 = (bf16[1,2048,352]{1,2,0:T(8,128)(2,1)S(1)}, bf16[1,2048,352]{1,2,0:T(8,128)(2,1)}, u32[]{:S(2)}) copy-start(bf16[1,2048,352]{1,2,0:T(8,128)(2,1)} %param.38) | copy-start | bytes 4325380
  191.2 6.1 %copy-start.12 = (bf16[32,1,2,32]{3,2,0,1:T(2,128)(2,1)S(1)}, bf16[32,1,2,32]{3,2,0,1:T(2,128)(2,1)}, u32[]{:S(2)}) copy-start(bf16[32,1,2,32]{3,2,0,1:T(2,128)(2,1)} %copy-done.11) | copy-start | bytes 12292
  191.2 6.9 %copy-start.18 = (f32[32,2]{0,1:T(2,128)S(1)}, f32[32,2]{0,1:T(2,128)}, u32[]{:S(2)}) copy-start(f32[32,2]{0,1:T(2,128)} %param.36) | copy-start | bytes 772
  192.7 23.6 %all-to-all-start.1 = ((bf16[16,16,1024]{2,1,0:T(8,128)(2,1)}), bf16[16,16,1024]{2,1,0:T(8,128)(2,1)S(1)}, u32[]{:S(2)}, u32[]{:S(2)}) async-start(bf16[16,16,1024]{2,1,0:T(8,128)(2,1)} %fusion.26), calls=%async_computation.1 | async-start | bytes 1048576 | tf_op jit(solution)/shard_map/all_to_all | solution.py:160
  (5 other events, 3.2 us)
Sparse Core Ops, SparseCore 0:
  65.5 75.4 all-gather.2
  148.7 86.8 reduce-scatter.1
